TPU v7x, 128 devices: a whole 4x4x4 slice. The times are simulated.
128 devices in a mesh: fs: 16 (over z, x), tp: 8 (over y, core).
Axes of the slice: x: 4, y: 4, z: 4, core: 2. Of those that a mesh axis runs over, the one named last changes fastest.
Arguments:
- tokens: bfloat16 [32, 384, 2048], P('fs', None, 'tp'), may hold values from -20 to 20
- first_gain: float32 [2048], replicated, may hold values from 0.1 to 1.9
- first_gate: bfloat16 [2048, 5120], P('fs', 'tp'), may hold values from -0.125 to 0.125
- first_up: bfloat16 [2048, 5120], P('fs', 'tp'), may hold values from -0.125 to 0.125
- first_down: bfloat16 [5120, 2048], P('tp', 'fs'), may hold values from -0.078125 to 0.078125
- mixer_gain: float32 [2048], replicated, may hold values from 0.1 to 1.9
- conv_input: bfloat16 [2048, 1024], P('fs', 'tp'), may hold values from -0.125 to 0.125
- outer_gate: bfloat16 [2048, 1024], P('fs', 'tp'), may hold values from -0.125 to 0.125
- inner_gate: bfloat16 [2048, 1024], P('fs', 'tp'), may hold values from -0.125 to 0.125
- conv_taps: float32 [3, 1024], P(None, 'tp'), may hold values from -3.5 to 3.5
- mixer_out: bfloat16 [1024, 2048], P('tp', 'fs'), may hold values from -0.1875 to 0.1875
- second_gain: float32 [2048], replicated, may hold values from 0.1 to 1.9
- second_gate: bfloat16 [2048, 5120], P('fs', 'tp'), may hold values from -0.125 to 0.125
- second_up: bfloat16 [2048, 5120], P('fs', 'tp'), may hold values from -0.125 to 0.125
- second_down: bfloat16 [5120, 2048], P('tp', 'fs'), may hold values from -0.078125 to 0.078125
Outputs:
- layer_out: bfloat16 [32, 384, 2048], P('fs', None, 'tp')
All inputs are finite; a program needn't handle non-finite values.
Results may differ from a plain program's by a relative error of at most 0.015.
Values may be sent and summed in bfloat16 or wider, within the bound.
A program may use at most 64 MiB of HBM per device.

v0:
```python
import jax
import jax.numpy as jnp
from jax import lax
from jax.sharding import PartitionSpec as P

epsilon = 1e-05


def sent_together(arrays, axis, dim, along):
    ends, at = ([], 0)
    for a in arrays[:-1]:
        at += a.shape[along]
        ends.append(at)
    both = jnp.concatenate(arrays, axis=along)
    return tuple(jnp.split(lax.all_gather(both, axis, axis=dim, tiled=True), ends, axis=along))


def copy_for_each(value, axis):
    copies = jnp.broadcast_to(value, (lax.axis_size(axis), *value.shape))
    return lax.all_to_all(copies, axis, split_axis=0, concat_axis=0, tiled=True)


def joined_along(pieces, dim):
    shape = list(pieces.shape[1:])
    shape[dim] *= pieces.shape[0]
    return jnp.moveaxis(pieces, 0, dim).reshape(shape)


def gathered_copies(value, axis, dim):
    pieces = copy_for_each(value, axis)
    return joined_along(pieces, dim)


def norm_rows(stream, gain):
    whole = lax.all_gather(stream, "tp", axis=1, tiled=True)
    values = whole.astype(jnp.float32)
    scale = lax.rsqrt(jnp.mean(values * values, axis=1, keepdims=True) + epsilon)
    return (values * scale * gain).astype(jnp.bfloat16)


def add_rows(gathered, piece):
    return jnp.dot(gathered, piece, preferred_element_type=jnp.float32)


def ffn_inputs(gathered, gate_weight, up_weight):
    pieces = sent_together((gate_weight, up_weight), "fs", 0, 1)
    gate = add_rows(gathered, pieces[0])
    upward = add_rows(gathered, pieces[1])
    return (gate, upward)


def mixer_inputs(gathered, conv_input, outer_gate, inner_gate):
    pieces = sent_together((conv_input, outer_gate, inner_gate), "fs", 0, 1)
    conv_values = add_rows(gathered, pieces[0])
    outer = add_rows(gathered, pieces[1])
    inner = add_rows(gathered, pieces[2])
    return (conv_values, outer, inner)


def project_down(hidden, weight):
    partial_sum = jnp.dot(
        hidden, gathered_copies(weight, "fs", 1), preferred_element_type=jnp.float32
    )
    result = lax.psum_scatter(
        partial_sum.astype(jnp.bfloat16), "tp", scatter_dimension=1, tiled=True
    ).astype(jnp.float32)
    return result


def half_ffn(stream, gain, gate_weight, up_weight, down_weight):
    gathered = norm_rows(stream, gain)
    gate, upward = ffn_inputs(gathered, gate_weight, up_weight)
    hidden = (jax.nn.silu(gate) * upward).astype(jnp.bfloat16)
    branch = project_down(hidden, down_weight)
    return (stream.astype(jnp.float32) + 0.5 * branch).astype(jnp.bfloat16)


def conv_mixer(stream, seqs, gain, conv_input, outer_gate, inner_gate, conv_taps, mixer_out):
    gathered = norm_rows(stream, gain)
    conv_values, outer, inner = mixer_inputs(gathered, conv_input, outer_gate, inner_gate)
    gated_input = (inner * conv_values).reshape(seqs, -1, conv_values.shape[1])
    one_back = jnp.pad(gated_input, ((0, 0), (1, 0), (0, 0)))[:, :-1]
    two_back = jnp.pad(gated_input, ((0, 0), (2, 0), (0, 0)))[:, :-2]
    convolved = conv_taps[0] * two_back + conv_taps[1] * one_back + conv_taps[2] * gated_input
    mixed = (outer * convolved.reshape(conv_values.shape)).astype(jnp.bfloat16)
    branch = project_down(mixed, mixer_out)
    return (stream.astype(jnp.float32) + branch).astype(jnp.bfloat16)


def on_device(
    tokens,
    first_gain,
    first_gate,
    first_up,
    first_down,
    mixer_gain,
    conv_input,
    outer_gate,
    inner_gate,
    conv_taps,
    mixer_out,
    second_gain,
    second_gate,
    second_up,
    second_down,
):
    seqs, length, width = tokens.shape
    stream = tokens.reshape(seqs * length, width)
    stream = half_ffn(stream, first_gain, first_gate, first_up, first_down)
    stream = conv_mixer(
        stream, seqs, mixer_gain, conv_input, outer_gate, inner_gate, conv_taps, mixer_out
    )
    stream = half_ffn(stream, second_gain, second_gate, second_up, second_down)
    return stream.reshape(seqs, length, width)


def solution(mesh):
    in_specs = (
        P("fs", None, "tp"),
        P(),
        P("fs", "tp"),
        P("fs", "tp"),
        P("tp", "fs"),
        P(),
        P("fs", "tp"),
        P("fs", "tp"),
        P("fs", "tp"),
        P(None, "tp"),
        P("tp", "fs"),
        P(),
        P("fs", "tp"),
        P("fs", "tp"),
        P("tp", "fs"),
    )
    out_specs = P("fs", None, "tp")
    return jax.shard_map(
        on_device, mesh=mesh, in_specs=in_specs, out_specs=out_specs, check_vma=False
    )
```

profile of v0, /device:TPU:0, one launch (start us, length us, event | category | flops | bytes accessed | tf_op | source)
XLA Modules:
  0.0 431.1 jit_solution(13457404551450091952)
XLA Ops:
  10.1 1.9 broadcast_in_dim.6
  12.0 8.2 %all-to-all-start = ((bf16[16,640,128]{1,2,0:T(8,128)(2,1)}), bf16[16,640,128]{1,2,0:T(8,128)(2,1)}, u32[]{:S(2)}, u32[]{:S(2)}) async-start(bf16[16,640,128]{1,2,0:T(8,128)(2,1)} %broadcast_in_dim.6), calls=%async_computation | async-start | bytes 5242880 | tf_op jit(solution)/shard_map/all_to_all | solution.py:20
  20.3 22.4 %all-gather.7.cloned.1.call-done = bf16[768,2048]{1,0:T(8,128)(2,1)} async-done(((bf16[768,256]{1,0:T(8,128)(2,1)}), bf16[768,2048]{1,0:T(8,128)(2,1)}) %all-gather.7.cloned.1.call-update) | async-done | bytes 3145744 | tf_op jit(solution)/shard_map/all_gather | solution.py:35
  42.7 2.7 fusion
  45.4 56.7 %all-gather.9.cloned.1.call-done = bf16[2048,1280]{1,0:T(8,128)(2,1)} async-done(((bf16[128,1280]{1,0:T(8,128)(2,1)}), bf16[2048,1280]{1,0:T(8,128)(2,1)}) %all-gather.9.cloned.1.call-update) | async-done | bytes 5242896 | tf_op jit(solution)/shard_map/all_gather | solution.py:15
  102.1 5.7 %fusion.15 = f32[768,640]{1,0:T(8,128)} fusion(bf16[2048,1280]{1,0:T(8,128)(2,1)} %all-gather.9.cloned.1.call-done, bf16[768,2048]{1,0:T(8,128)(2,1)S(1)} %copy-done.3, f32[2048]{0:T(1024)S(1)} %copy-done.15, f32[768]{0:T(1024)S(1)} %add_rsqrt_fusion.2), kind=kOutput, calls=%fused_computation.24 | convolution fusion | flops 2019557376 | bytes 7744512 | tf_op jit(solution)/shard_map/dot_general | solution.py:42
  107.8 10.7 %convolution_convert_fusion.1 = bf16[768,2048]{1,0:T(8,128)(2,1)} fusion(bf16[640,2048]{0,1:T(8,128)(2,1)} %bitcast.2, f32[768,640]{1,0:T(8,128)} %fusion.15, bf16[2048,1280]{1,0:T(8,128)(2,1)} %all-gather.9.cloned.1.call-done, bf16[768,2048]{1,0:T(8,128)(2,1)S(1)} %copy-done.3, f32[2048]{0:T(1024)S(1)} %copy-done.15, f32[768]{0:T(1024)S(1)} %add_rsqrt_fusion.2), kind=kOutput, calls=%fused_computation.16 | convolution fusion | flops 4037345280 | bytes 13511680 | tf_op jit(solution)/shard_map/dot_general | solution.py:61
  118.6 35.6 %reduce-scatter.4.cloned.1.call-done = bf16[768,256]{1,0:T(8,128)(2,1)} async-done(((bf16[768,2048]{1,0:T(8,128)(2,1)}), bf16[768,256]{1,0:T(8,128)(2,1)}) %reduce-scatter.4.cloned.1.call-update) | async-done | bytes 393232 | tf_op jit(solution)/shard_map/reduce_scatter | solution.py:64
  157.9 7.0 %all-to-all-start.1 = ((bf16[16,128,128]{1,2,0:T(8,128)(2,1)}), bf16[16,128,128]{1,2,0:T(8,128)(2,1)}, u32[]{:S(2)}, u32[]{:S(2)}) async-start(bf16[16,128,128]{1,2,0:T(8,128)(2,1)} %broadcast_in_dim.7), calls=%async_computation.2 | async-start | bytes 1048576 | tf_op jit(solution)/shard_map/all_to_all | solution.py:20
  165.2 21.0 %all-gather.11.cloned.1.call-done = bf16[768,2048]{1,0:T(8,128)(2,1)} async-done(((bf16[768,256]{1,0:T(8,128)(2,1)}), bf16[768,2048]{1,0:T(8,128)(2,1)}) %all-gather.11.cloned.1.call-update) | async-done | bytes 3145744 | tf_op jit(solution)/shard_map/all_gather | solution.py:35
  186.2 2.7 fusion.3
  189.8 43.1 %all-gather.13.cloned.1.call-done = bf16[2048,384]{1,0:T(8,128)(2,1)} async-done(((bf16[128,384]{1,0:T(8,128)(2,1)}), bf16[2048,384]{1,0:T(8,128)(2,1)}) %all-gather.13.cloned.1.call-update) | async-done | bytes 1572880 | tf_op jit(solution)/shard_map/all_gather | solution.py:15
  233.0 2.0 fusion.35
  235.0 2.0 convolution_multiply_fusion
  237.1 6.2 %convolution_convert_fusion.2 = bf16[768,2048]{1,0:T(8,128)(2,1)} fusion(bf16[128,2048]{0,1:T(8,128)(2,1)} %bitcast.9, f32[768,128]{1,0:T(8,128)S(1)} %bitcast.28, bf16[768,2048]{1,0:T(8,128)(2,1)S(1)} %fusion.5, bf16[2048,384]{1,0:T(8,128)(2,1)} %all-gather.13.cloned.1.call-done), kind=kOutput, calls=%fused_computation.17 | convolution fusion | flops 807075840 | bytes 7733248 | tf_op jit(solution)/shard_map/dot_general | solution.py:61
  243.4 35.3 %reduce-scatter.6.cloned.1.call-done = bf16[768,256]{1,0:T(8,128)(2,1)} async-done(((bf16[768,2048]{1,0:T(8,128)(2,1)}), bf16[768,256]{1,0:T(8,128)(2,1)}) %reduce-scatter.6.cloned.1.call-update) | async-done | bytes 393232 | tf_op jit(solution)/shard_map/reduce_scatter | solution.py:64
  281.6 1.9 broadcast_in_dim.8
  283.5 7.1 %all-to-all-start.2 = ((bf16[16,640,128]{1,2,0:T(8,128)(2,1)}), bf16[16,640,128]{1,2,0:T(8,128)(2,1)}, u32[]{:S(2)}, u32[]{:S(2)}) async-start(bf16[16,640,128]{1,2,0:T(8,128)(2,1)} %broadcast_in_dim.8), calls=%async_computation.4 | async-start | bytes 5242880 | tf_op jit(solution)/shard_map/all_to_all | solution.py:20
  290.9 19.8 %all-gather.15.cloned.1.call-done = bf16[768,2048]{1,0:T(8,128)(2,1)} async-done(((bf16[768,256]{1,0:T(8,128)(2,1)}), bf16[768,2048]{1,0:T(8,128)(2,1)}) %all-gather.15.cloned.1.call-update) | async-done | bytes 3145744 | tf_op jit(solution)/shard_map/all_gather | solution.py:35
  310.7 2.7 fusion.6
  313.4 57.2 %all-gather.17.cloned.1.call-done = bf16[2048,1280]{1,0:T(8,128)(2,1)} async-done(((bf16[128,1280]{1,0:T(8,128)(2,1)}), bf16[2048,1280]{1,0:T(8,128)(2,1)}) %all-gather.17.cloned.1.call-update) | async-done | bytes 5242896 | tf_op jit(solution)/shard_map/all_gather | solution.py:15
  370.6 5.7 %fusion.11 = f32[768,640]{1,0:T(8,128)} fusion(bf16[2048,1280]{1,0:T(8,128)(2,1)} %all-gather.17.cloned.1.call-done, bf16[768,2048]{1,0:T(8,128)(2,1)S(1)} %copy-done.4, f32[2048]{0:T(1024)S(1)} %copy-done.16, f32[768]{0:T(1024)S(1)} %add_rsqrt_fusion), kind=kOutput, calls=%fused_computation.20 | convolution fusion | flops 2019557376 | bytes 7744512 | tf_op jit(solution)/shard_map/dot_general | solution.py:42
  376.3 10.7 %convolution_convert_fusion = bf16[768,2048]{1,0:T(8,128)(2,1)} fusion(bf16[640,2048]{0,1:T(8,128)(2,1)} %bitcast.11, f32[768,640]{1,0:T(8,128)} %fusion.11, bf16[2048,1280]{1,0:T(8,128)(2,1)} %all-gather.17.cloned.1.call-done, bf16[768,2048]{1,0:T(8,128)(2,1)S(1)} %copy-done.4, f32[2048]{0:T(1024)S(1)} %copy-done.16, f32[768]{0:T(1024)S(1)} %add_rsqrt_fusion), kind=kOutput, calls=%fused_computation.15 | convolution fusion | flops 4037345280 | bytes 13511680 | tf_op jit(solution)/shard_map/dot_general | solution.py:61
  387.0 35.7 %reduce-scatter.8.cloned.1.call-done = bf16[768,256]{1,0:T(8,128)(2,1)} async-done(((bf16[768,2048]{1,0:T(8,128)(2,1)}), bf16[768,256]{1,0:T(8,128)(2,1)}) %reduce-scatter.8.cloned.1.call-update) | async-done | bytes 393232 | tf_op jit(solution)/shard_map/reduce_scatter | solution.py:64
  (71 shorter events, 13.6 us)
Async XLA Ops:
  6.5 36.1 %all-gather.7.cloned.1.call-start = ((), (), s32[]{:S(2)}) async-start(), calls=%async_computation.6 | async-start | bytes 3538944 | tf_op jit(solution)/shard_map/all_gather | solution.py:35
  7.3 94.8 %all-gather.9.cloned.1.call-start = ((), (), s32[]{:S(2)}) async-start(), calls=%async_computation.7 | async-start | bytes 5570560 | tf_op jit(solution)/shard_map/all_gather | solution.py:15
  12.0 90.1 %copy-start.15 = (f32[2048]{0:T(1024)S(1)}, f32[2048]{0:T(1024)}, u32[]{:S(2)}) copy-start(f32[2048]{0:T(1024)} %param.16) | copy-start | bytes 24580
  12.0 95.8 %all-to-all-start = ((bf16[16,640,128]{1,2,0:T(8,128)(2,1)}), bf16[16,640,128]{1,2,0:T(8,128)(2,1)}, u32[]{:S(2)}, u32[]{:S(2)}) async-start(bf16[16,640,128]{1,2,0:T(8,128)(2,1)} %broadcast_in_dim.6), calls=%async_computation | async-start | bytes 5242880 | tf_op jit(solution)/shard_map/all_to_all | solution.py:20
  20.2 134.0 %reduce-scatter.4.cloned.1.call-start = ((), (), s32[]{:S(2)}) async-start(), calls=%async_computation.8 | async-start | bytes 3538944 | tf_op jit(solution)/shard_map/reduce_scatter | solution.py:64
  42.7 59.5 %copy-start.3 = (bf16[768,2048]{1,0:T(8,128)(2,1)S(1)}, bf16[768,2048]{1,0:T(8,128)(2,1)}, u32[]{:S(2)}) copy-start(bf16[768,2048]{1,0:T(8,128)(2,1)} %all-gather.7.cloned.1.call-done) | copy-start | bytes 9437188
  118.5 37.7 %copy-start.10 = (bf16[128,128]{1,0:T(8,128)(2,1)S(1)}, bf16[128,128]{1,0:T(8,128)(2,1)}, u32[]{:S(2)}) copy-start(bf16[128,128]{1,0:T(8,128)(2,1)} %param.23) | copy-start | bytes 98308
  118.5 37.7 %copy-start.11 = (bf16[128,128]{1,0:T(8,128)(2,1)S(1)}, bf16[128,128]{1,0:T(8,128)(2,1)}, u32[]{:S(2)}) copy-start(bf16[128,128]{1,0:T(8,128)(2,1)} %param.22) | copy-start | bytes 98308
  118.5 37.7 %copy-start.12 = (bf16[128,128]{1,0:T(8,128)(2,1)S(1)}, bf16[128,128]{1,0:T(8,128)(2,1)}, u32[]{:S(2)}) copy-start(bf16[128,128]{1,0:T(8,128)(2,1)} %param.21) | copy-start | bytes 98308
  118.5 38.3 %copy-start.9 = (bf16[128,128]{1,0:T(8,128)(2,1)S(1)}, bf16[128,128]{1,0:T(8,128)(2,1)}, u32[]{:S(2)}) copy-start(bf16[128,128]{1,0:T(8,128)(2,1)} %param.25) | copy-start | bytes 98308
  118.5 46.6 %copy-start.14 = (f32[3,128]{1,0:T(4,128)S(1)}, f32[3,128]{1,0:T(4,128)}, u32[]{:S(2)}) copy-start(f32[3,128]{1,0:T(4,128)} %param.24) | copy-start | bytes 4612
  118.5 70.4 %copy-start.13 = (f32[2048]{0:T(1024)S(1)}, f32[2048]{0:T(1024)}, u32[]{:S(2)}) copy-start(f32[2048]{0:T(1024)} %param.20) | copy-start | bytes 24580
  118.6 67.6 %all-gather.11.cloned.1.call-start = ((), (), s32[]{:S(2)}) async-start(), calls=%async_computation.9 | async-start | bytes 3538944 | tf_op jit(solution)/shard_map/all_gather | solution.py:35
  156.1 76.9 %all-gather.13.cloned.1.call-start = ((), (), s32[]{:S(2)}) async-start(), calls=%async_computation.10 | async-start | bytes 1671168 | tf_op jit(solution)/shard_map/all_gather | solution.py:15
  157.9 79.2 %all-to-all-start.1 = ((bf16[16,128,128]{1,2,0:T(8,128)(2,1)}), bf16[16,128,128]{1,2,0:T(8,128)(2,1)}, u32[]{:S(2)}, u32[]{:S(2)}) async-start(bf16[16,128,128]{1,2,0:T(8,128)(2,1)} %broadcast_in_dim.7), calls=%async_computation.2 | async-start | bytes 1048576 | tf_op jit(solution)/shard_map/all_to_all | solution.py:20
  164.9 113.8 %reduce-scatter.6.cloned.1.call-start = ((), (), s32[]{:S(2)}) async-start(), calls=%async_computation.11 | async-start | bytes 3538944 | tf_op jit(solution)/shard_map/reduce_scatter | solution.py:64
  243.3 37.3 %copy-start.7 = (bf16[128,640]{1,0:T(8,128)(2,1)S(1)}, bf16[128,640]{1,0:T(8,128)(2,1)}, u32[]{:S(2)}) copy-start(bf16[128,640]{1,0:T(8,128)(2,1)} %param.27) | copy-start | bytes 491524
  243.3 38.1 %copy-start.8 = (bf16[640,128]{1,0:T(8,128)(2,1)S(1)}, bf16[640,128]{1,0:T(8,128)(2,1)}, u32[]{:S(2)}) copy-start(bf16[640,128]{1,0:T(8,128)(2,1)} %param.29) | copy-start | bytes 491524
  243.3 67.3 %all-gather.15.cloned.1.call-start = ((), (), s32[]{:S(2)}) async-start(), calls=%async_computation.12 | async-start | bytes 3538944 | tf_op jit(solution)/shard_map/all_gather | solution.py:35
  280.6 90.0 %all-gather.17.cloned.1.call-start = ((), (), s32[]{:S(2)}) async-start(), calls=%async_computation.13 | async-start | bytes 5570560 | tf_op jit(solution)/shard_map/all_gather | solution.py:15
  283.5 87.1 %copy-start.16 = (f32[2048]{0:T(1024)S(1)}, f32[2048]{0:T(1024)}, u32[]{:S(2)}) copy-start(f32[2048]{0:T(1024)} %param.26) | copy-start | bytes 24580
  283.5 92.8 %all-to-all-start.2 = ((bf16[16,640,128]{1,2,0:T(8,128)(2,1)}), bf16[16,640,128]{1,2,0:T(8,128)(2,1)}, u32[]{:S(2)}, u32[]{:S(2)}) async-start(bf16[16,640,128]{1,2,0:T(8,128)(2,1)} %broadcast_in_dim.8), calls=%async_computation.4 | async-start | bytes 5242880 | tf_op jit(solution)/shard_map/all_to_all | solution.py:20
  290.6 132.1 %reduce-scatter.8.cloned.1.call-start = ((), (), s32[]{:S(2)}) async-start(), calls=%async_computation.14 | async-start | bytes 3538944 | tf_op jit(solution)/shard_map/reduce_scatter | solution.py:64
  310.7 60.0 %copy-start.4 = (bf16[768,2048]{1,0:T(8,128)(2,1)S(1)}, bf16[768,2048]{1,0:T(8,128)(2,1)}, u32[]{:S(2)}) copy-start(bf16[768,2048]{1,0:T(8,128)(2,1)} %all-gather.15.cloned.1.call-done) | copy-start | bytes 9437188
  (5 other events, 147.0 us)
Sparse Core Ops, SparseCore 0:
  9.0 33.5 all-gather.6
  44.8 57.2 all-gather.8
  118.7 35.4 reduce-scatter.3
  156.2 29.9 all-gather.10
  188.2 44.7 all-gather.12
  243.5 35.2 reduce-scatter.5
  280.7 29.9 all-gather.14
  312.8 57.7 all-gather.16
  387.1 35.4 reduce-scatter.7
where the time goes:
time: 432 us; the launch traced here: 431 us
  waiting for transfers between devices  328 us (76%)
  matrix products  42.9 us (10%)
  starting transfers between devices  23 us (5%)
  other arithmetic  17.8 us (4%)
  between operations  13.4 us (3%)
  local copies, waits for them, and re-layouts  6.23 us (1%)
    all_gather x3, waiting for transfers between devices, sent_together(): lax.all_gather(both, axis, axis=dim, tiled=True)  157 us
    reduce_scatter x3, waiting for transfers between devices, project_down(): lax.psum_scatter(partial_sum.astype(jnp.bfloat16), 'tp', scatter_dimensio...  107 us
    all_gather x3, waiting for transfers between devices, norm_rows(): whole = lax.all_gather(stream, 'tp', axis=1, tiled=True)  63.2 us
    dot_general x3, matrix products, project_down(): jnp.dot(hidden, gathered_copies(weight, 'fs', 1), preferred_element_type=...  27.5 us
    all_to_all x3, starting transfers between devices, copy_for_each(): return lax.all_to_all(copies, axis, split_axis=0, concat_axis=0, tiled=True)  22.3 us
    dot_general x4, matrix products, add_rows(): return jnp.dot(gathered, piece, preferred_element_type=jnp.float32)  15.4 us
  transfers between devices with their start and end apart: 12, of which 9 were waited for; matrix products, arithmetic and copies ran while one was open for 8% of the time, Pallas kernels for 0%

commit v1 on v0

--- a/solution.py
+++ b/solution.py
@@ -32,7 +32,16 @@
 
 
 def norm_rows(stream, gain):
-    whole = lax.all_gather(stream, "tp", axis=1, tiled=True)
+    parts_n = jax.lax.axis_size("tp")
+    windows = [(rr, (rr + 1) % parts_n) for rr in range(parts_n)]
+    all_blocks = [(rr, (rr - 1) % parts_n) for rr in range(parts_n)]
+    arr_next, spare = ([stream], [stream])
+    for _ in range(parts_n // 2):
+        arr_next.append(jax.lax.ppermute(arr_next[-1], "tp", windows))
+    for _ in range((parts_n - 1) // 2):
+        spare.append(jax.lax.ppermute(spare[-1], "tp", all_blocks))
+    m_next = jnp.concatenate([*arr_next[::-1], *spare[1:]], axis=1)
+    whole = jnp.roll(m_next, (jax.lax.axis_index("tp") - parts_n // 2) * stream.shape[1], axis=1)
     values = whole.astype(jnp.float32)
     scale = lax.rsqrt(jnp.mean(values * values, axis=1, keepdims=True) + epsilon)
     return (values * scale * gain).astype(jnp.bfloat16)

time: 432 us -> 406 us (0.940)
  waiting for transfers between devices: 328 us -> 274 us
  starting transfers between devices: 23 us -> 49.3 us
    ppermute x0 -> x21, waiting for transfers between devices: none -> 71.5 us  [the longest x12 56.1 us: norm_rows(): arr_next.append(jax.lax.ppermute(arr_next[-1], 'tp', windows))]
    all_gather x3, waiting for transfers between devices: 157 us -> 91.8 us  [sent_together(): lax.all_gather(both, axis, axis=dim, tiled=True)]
    all_gather x3 -> x0, waiting for transfers between devices: 63.2 us -> none  [norm_rows(): whole = lax.all_gather(stream, 'tp', axis=1, tiled=True)]
    ppermute x0 -> x21, starting transfers between devices: none -> 26.5 us  [the longest x9 26.4 us: norm_rows(): spare.append(jax.lax.ppermute(spare[-1], 'tp', all_blocks))]
  transfers between devices with their start and end apart: 12 -> 30, of which waited for: 9 -> 20; matrix products, arithmetic and copies ran while one was open for 8% -> 9% of each run, Pallas kernels for 0% -> 0%
where the time goes in v1:
time: 406 us; the launch traced here: 405 us
  waiting for transfers between devices  274 us (67%)
  starting transfers between devices  49.3 us (12%)
  matrix products  43.4 us (11%)
  other arithmetic  16.6 us (4%)
  between operations  13.9 us (3%)
  local copies, waits for them, and re-layouts  7.94 us (2%)
    reduce_scatter x3, waiting for transfers between devices, project_down(): lax.psum_scatter(partial_sum.astype(jnp.bfloat16), 'tp', scatter_dimensio...  110 us
    all_gather x3, waiting for transfers between devices, sent_together(): lax.all_gather(both, axis, axis=dim, tiled=True)  91.8 us
    ppermute x12, waiting for transfers between devices, norm_rows(): arr_next.append(jax.lax.ppermute(arr_next[-1], 'tp', windows))  56.1 us
    dot_general x3, matrix products, project_down(): jnp.dot(hidden, gathered_copies(weight, 'fs', 1), preferred_element_type=...  27.8 us
    ppermute x9, starting transfers between devices, norm_rows(): spare.append(jax.lax.ppermute(spare[-1], 'tp', all_blocks))  26.4 us
    all_to_all x3, starting transfers between devices, copy_for_each(): return lax.all_to_all(copies, axis, split_axis=0, concat_axis=0, tiled=True)  22.1 us
    dot_general x4, matrix products, add_rows(): return jnp.dot(gathered, piece, preferred_element_type=jnp.float32)  15.6 us
    ppermute x9, waiting for transfers between devices, norm_rows(): spare.append(jax.lax.ppermute(spare[-1], 'tp', all_blocks))  15.4 us
  transfers between devices with their start and end apart: 30, of which 20 were waited for; matrix products, arithmetic and copies ran while one was open for 9% of the time, Pallas kernels for 0%

profile of v1, /device:TPU:0, one launch (start us, length us, event | category | flops | bytes accessed | tf_op | source)
XLA Modules:
  0.0 404.8 jit_solution(12831776776340467285)
XLA Ops:
  8.3 8.6 %collective-permute-done = bf16[768,256]{1,0:T(8,128)(2,1)S(1)} collective-permute-done((bf16[768,256]{1,0:T(8,128)(2,1)}, bf16[768,256]{1,0:T(8,128)(2,1)S(1)}, u32[]{:S(2)}, u32[]{:S(2)}) %collective-permute-start) | collective-permute-done | bytes 393248 | tf_op jit(solution)/shard_map/ppermute | solution.py:40
  19.9 5.5 %collective-permute-done.1 = bf16[768,256]{1,0:T(8,128)(2,1)S(1)} collective-permute-done((bf16[768,256]{1,0:T(8,128)(2,1)S(1)}, bf16[768,256]{1,0:T(8,128)(2,1)S(1)}, u32[]{:S(2)}, u32[]{:S(2)}) %collective-permute-start.1) | collective-permute-done | bytes 393248 | tf_op jit(solution)/shard_map/ppermute | solution.py:40
  28.9 4.8 %collective-permute-done.2 = bf16[768,256]{1,0:T(8,128)(2,1)S(1)} collective-permute-done((bf16[768,256]{1,0:T(8,128)(2,1)S(1)}, bf16[768,256]{1,0:T(8,128)(2,1)S(1)}, u32[]{:S(2)}, u32[]{:S(2)}) %collective-permute-start.2) | collective-permute-done | bytes 393248 | tf_op jit(solution)/shard_map/ppermute | solution.py:40
  36.6 8.2 %all-to-all-start = ((bf16[16,640,128]{1,2,0:T(8,128)(2,1)}), bf16[16,640,128]{1,2,0:T(8,128)(2,1)}, u32[]{:S(2)}, u32[]{:S(2)}) async-start(bf16[16,640,128]{1,2,0:T(8,128)(2,1)} %broadcast_in_dim.6), calls=%async_computation | async-start | bytes 5242880 | tf_op jit(solution)/shard_map/all_to_all | solution.py:20
  48.0 4.9 %collective-permute-done.6 = bf16[768,256]{1,0:T(8,128)(2,1)S(1)} collective-permute-done((bf16[768,256]{1,0:T(8,128)(2,1)S(1)}, bf16[768,256]{1,0:T(8,128)(2,1)S(1)}, u32[]{:S(2)}, u32[]{:S(2)}) %collective-permute-start.6) | collective-permute-done | bytes 393248 | tf_op jit(solution)/shard_map/ppermute | solution.py:42
  55.2 42.7 %all-gather.4.cloned.1.call-done = bf16[2048,1280]{1,0:T(8,128)(2,1)} async-done(((bf16[128,1280]{1,0:T(8,128)(2,1)}), bf16[2048,1280]{1,0:T(8,128)(2,1)}) %all-gather.4.cloned.1.call-update) | async-done | bytes 5242896 | tf_op jit(solution)/shard_map/all_gather | solution.py:15
  97.9 5.8 %fusion.16 = f32[768,640]{1,0:T(8,128)} fusion(bf16[2048,1280]{1,0:T(8,128)(2,1)} %all-gather.4.cloned.1.call-done, bf16[768,2048]{1,0:T(8,128)(2,1)S(1)} %get-tuple-element.9, f32[2048]{0:T(1024)S(1)} %copy-done.11, f32[768]{0:T(1024)S(1)} %add_rsqrt_fusion.2), kind=kOutput, calls=%fused_computation.31 | convolution fusion | flops 2019557376 | bytes 7744512 | tf_op jit(solution)/shard_map/dot_general | solution.py:51
  103.7 10.7 %convolution_convert_fusion.1 = bf16[768,2048]{1,0:T(8,128)(2,1)} fusion(bf16[640,2048]{0,1:T(8,128)(2,1)} %bitcast.2, f32[768,640]{1,0:T(8,128)} %fusion.16, bf16[2048,1280]{1,0:T(8,128)(2,1)} %all-gather.4.cloned.1.call-done, bf16[768,2048]{1,0:T(8,128)(2,1)S(1)} %get-tuple-element.9, f32[2048]{0:T(1024)S(1)} %copy-done.11, f32[768]{0:T(1024)S(1)} %add_rsqrt_fusion.2), kind=kOutput, calls=%fused_computation.22 | convolution fusion | flops 4037345280 | bytes 13511680 | tf_op jit(solution)/shard_map/dot_general | solution.py:70
  114.5 37.2 %reduce-scatter.4.cloned.1.call-done = bf16[768,256]{1,0:T(8,128)(2,1)} async-done(((bf16[768,2048]{1,0:T(8,128)(2,1)}), bf16[768,256]{1,0:T(8,128)(2,1)}) %reduce-scatter.4.cloned.1.call-update) | async-done | bytes 393232 | tf_op jit(solution)/shard_map/reduce_scatter | solution.py:73
  152.9 8.4 %collective-permute-done.7 = bf16[768,256]{1,0:T(8,128)(2,1)S(1)} collective-permute-done((bf16[768,256]{1,0:T(8,128)(2,1)S(1)}, bf16[768,256]{1,0:T(8,128)(2,1)S(1)}, u32[]{:S(2)}, u32[]{:S(2)}) %collective-permute-start.7) | collective-permute-done | bytes 393248 | tf_op jit(solution)/shard_map/ppermute | solution.py:40
  179.2 7.0 %all-to-all-start.1 = ((bf16[16,128,128]{1,2,0:T(8,128)(2,1)}), bf16[16,128,128]{1,2,0:T(8,128)(2,1)}, u32[]{:S(2)}, u32[]{:S(2)}) async-start(bf16[16,128,128]{1,2,0:T(8,128)(2,1)} %broadcast_in_dim.7), calls=%async_computation.2 | async-start | bytes 1048576 | tf_op jit(solution)/shard_map/all_to_all | solution.py:20
  189.5 4.9 %collective-permute-done.13 = bf16[768,256]{1,0:T(8,128)(2,1)S(1)} collective-permute-done((bf16[768,256]{1,0:T(8,128)(2,1)S(1)}, bf16[768,256]{1,0:T(8,128)(2,1)S(1)}, u32[]{:S(2)}, u32[]{:S(2)}) %collective-permute-start.13) | collective-permute-done | bytes 393248 | tf_op jit(solution)/shard_map/ppermute | solution.py:42
  198.5 11.9 %all-gather.6.cloned.1.call-done = bf16[2048,384]{1,0:T(8,128)(2,1)} async-done(((bf16[128,384]{1,0:T(8,128)(2,1)}), bf16[2048,384]{1,0:T(8,128)(2,1)}) %all-gather.6.cloned.1.call-update) | async-done | bytes 1572880 | tf_op jit(solution)/shard_map/all_gather | solution.py:15
  215.3 6.4 %convolution_convert_fusion.2 = bf16[768,2048]{1,0:T(8,128)(2,1)} fusion(bf16[128,2048]{0,1:T(8,128)(2,1)} %bitcast.9, f32[768,128]{1,0:T(8,128)} %bitcast.30, bf16[768,2048]{1,0:T(8,128)(2,1)S(1)} %fusion.5, bf16[2048,384]{1,0:T(8,128)(2,1)} %all-gather.6.cloned.1.call-done), kind=kOutput, calls=%fused_computation.23 | convolution fusion | flops 807075840 | bytes 7733248 | tf_op jit(solution)/shard_map/dot_general | solution.py:70
  223.4 33.6 %reduce-scatter.6.cloned.1.call-done = bf16[768,256]{1,0:T(8,128)(2,1)} async-done(((bf16[768,2048]{1,0:T(8,128)(2,1)}), bf16[768,256]{1,0:T(8,128)(2,1)}) %reduce-scatter.6.cloned.1.call-update) | async-done | bytes 393232 | tf_op jit(solution)/shard_map/reduce_scatter | solution.py:73
  258.1 8.4 %collective-permute-done.14 = bf16[768,256]{1,0:T(8,128)(2,1)S(1)} collective-permute-done((bf16[768,256]{1,0:T(8,128)(2,1)S(1)}, bf16[768,256]{1,0:T(8,128)(2,1)S(1)}, u32[]{:S(2)}, u32[]{:S(2)}) %collective-permute-start.14) | collective-permute-done | bytes 393248 | tf_op jit(solution)/shard_map/ppermute | solution.py:40
  269.5 5.5 %collective-permute-done.15 = bf16[768,256]{1,0:T(8,128)(2,1)S(1)} collective-permute-done((bf16[768,256]{1,0:T(8,128)(2,1)S(1)}, bf16[768,256]{1,0:T(8,128)(2,1)S(1)}, u32[]{:S(2)}, u32[]{:S(2)}) %collective-permute-start.15) | collective-permute-done | bytes 393248 | tf_op jit(solution)/shard_map/ppermute | solution.py:40
  277.9 5.4 %collective-permute-done.16 = bf16[768,256]{1,0:T(8,128)(2,1)S(1)} collective-permute-done((bf16[768,256]{1,0:T(8,128)(2,1)S(1)}, bf16[768,256]{1,0:T(8,128)(2,1)S(1)}, u32[]{:S(2)}, u32[]{:S(2)}) %collective-permute-start.16) | collective-permute-done | bytes 393248 | tf_op jit(solution)/shard_map/ppermute | solution.py:40
  285.3 7.0 %all-to-all-start.2 = ((bf16[16,640,128]{1,2,0:T(8,128)(2,1)}), bf16[16,640,128]{1,2,0:T(8,128)(2,1)}, u32[]{:S(2)}, u32[]{:S(2)}) async-start(bf16[16,640,128]{1,2,0:T(8,128)(2,1)} %broadcast_in_dim.8), calls=%async_computation.4 | async-start | bytes 5242880 | tf_op jit(solution)/shard_map/all_to_all | solution.py:20
  295.6 4.9 %collective-permute-done.20 = bf16[768,256]{1,0:T(8,128)(2,1)S(1)} collective-permute-done((bf16[768,256]{1,0:T(8,128)(2,1)S(1)}, bf16[768,256]{1,0:T(8,128)(2,1)S(1)}, u32[]{:S(2)}, u32[]{:S(2)}) %collective-permute-start.20) | collective-permute-done | bytes 393248 | tf_op jit(solution)/shard_map/ppermute | solution.py:42
  302.9 37.2 %all-gather.8.cloned.1.call-done = bf16[2048,1280]{1,0:T(8,128)(2,1)} async-done(((bf16[128,1280]{1,0:T(8,128)(2,1)}), bf16[2048,1280]{1,0:T(8,128)(2,1)}) %all-gather.8.cloned.1.call-update) | async-done | bytes 5242896 | tf_op jit(solution)/shard_map/all_gather | solution.py:15
  340.1 5.8 %fusion.12 = f32[768,640]{1,0:T(8,128)} fusion(bf16[2048,1280]{1,0:T(8,128)(2,1)} %all-gather.8.cloned.1.call-done, bf16[768,2048]{1,0:T(8,128)(2,1)S(1)} %get-tuple-element.7, f32[2048]{0:T(1024)S(1)} %copy-done.12, f32[768]{0:T(1024)S(1)} %add_rsqrt_fusion), kind=kOutput, calls=%fused_computation.27 | convolution fusion | flops 2019557376 | bytes 7744512 | tf_op jit(solution)/shard_map/dot_general | solution.py:51
  345.9 10.7 %convolution_convert_fusion = bf16[768,2048]{1,0:T(8,128)(2,1)} fusion(bf16[640,2048]{0,1:T(8,128)(2,1)} %bitcast.11, f32[768,640]{1,0:T(8,128)} %fusion.12, bf16[2048,1280]{1,0:T(8,128)(2,1)} %all-gather.8.cloned.1.call-done, bf16[768,2048]{1,0:T(8,128)(2,1)S(1)} %get-tuple-element.7, f32[2048]{0:T(1024)S(1)} %copy-done.12, f32[768]{0:T(1024)S(1)} %add_rsqrt_fusion), kind=kOutput, calls=%fused_computation.21 | convolution fusion | flops 4037345280 | bytes 13511680 | tf_op jit(solution)/shard_map/dot_general | solution.py:70
  356.6 39.5 %reduce-scatter.8.cloned.1.call-done = bf16[768,256]{1,0:T(8,128)(2,1)} async-done(((bf16[768,2048]{1,0:T(8,128)(2,1)}), bf16[768,256]{1,0:T(8,128)(2,1)}) %reduce-scatter.8.cloned.1.call-update) | async-done | bytes 393232 | tf_op jit(solution)/shard_map/reduce_scatter | solution.py:73
  (120 shorter events, 66.1 us)
Async XLA Ops:
  6.5 91.4 %all-gather.4.cloned.1.call-start = ((), (), s32[]{:S(2)}) async-start(), calls=%async_computation.6 | async-start | bytes 5570560 | tf_op jit(solution)/shard_map/all_gather | solution.py:15
  8.3 8.6 %collective-permute-start = (bf16[768,256]{1,0:T(8,128)(2,1)}, bf16[768,256]{1,0:T(8,128)(2,1)S(1)}, u32[]{:S(2)}, u32[]{:S(2)}) collective-permute-start(bf16[768,256]{1,0:T(8,128)(2,1)} %bitcast.27), channel_id=1, source_target_pairs={{0,1},{1,2},{2,3},{3,4},{4,5},{5,6},{6,7},{7,0},{8,9},{9,10},{10,1... | collective-permute-start | bytes 1179656 | tf_op jit(solution)/shard_map/ppermute | solution.py:40
  16.9 8.4 %collective-permute-start.1 = (bf16[768,256]{1,0:T(8,128)(2,1)S(1)}, bf16[768,256]{1,0:T(8,128)(2,1)S(1)}, u32[]{:S(2)}, u32[]{:S(2)}) collective-permute-start(bf16[768,256]{1,0:T(8,128)(2,1)S(1)} %collective-permute-done), channel_id=1, source_target_pairs={{0,1},{1,2},{2,3},{3,4},{4,5},{5,6},{6,7},{7,0},{8,9},{9,10},{10,1... | collective-permute-start | bytes 1179656 | tf_op jit(solution)/shard_map/ppermute | solution.py:40
  16.9 8.6 %collective-permute-start.4 = (bf16[768,256]{1,0:T(8,128)(2,1)}, bf16[768,256]{1,0:T(8,128)(2,1)S(1)}, u32[]{:S(2)}, u32[]{:S(2)}) collective-permute-start(bf16[768,256]{1,0:T(8,128)(2,1)} %bitcast.28), channel_id=1, source_target_pairs={{0,7},{1,0},{2,1},{3,2},{4,3},{5,4},{6,5},{7,6},{8,15},{9,8},{10,9... | collective-permute-start | bytes 1179656 | tf_op jit(solution)/shard_map/ppermute | solution.py:42
  25.4 8.4 %collective-permute-start.2 = (bf16[768,256]{1,0:T(8,128)(2,1)S(1)}, bf16[768,256]{1,0:T(8,128)(2,1)S(1)}, u32[]{:S(2)}, u32[]{:S(2)}) collective-permute-start(bf16[768,256]{1,0:T(8,128)(2,1)S(1)} %collective-permute-done.1), channel_id=1, source_target_pairs={{0,1},{1,2},{2,3},{3,4},{4,5},{5,6},{6,7},{7,0},{8,9},{9,10},{10,1... | collective-permute-start | bytes 1179656 | tf_op jit(solution)/shard_map/ppermute | solution.py:40
  25.5 19.4 %collective-permute-start.5 = (bf16[768,256]{1,0:T(8,128)(2,1)S(1)}, bf16[768,256]{1,0:T(8,128)(2,1)S(1)}, u32[]{:S(2)}, u32[]{:S(2)}) collective-permute-start(bf16[768,256]{1,0:T(8,128)(2,1)S(1)} %collective-permute-done.4), channel_id=1, source_target_pairs={{0,7},{1,0},{2,1},{3,2},{4,3},{5,4},{6,5},{7,6},{8,15},{9,8},{10,9... | collective-permute-start | bytes 1179656 | tf_op jit(solution)/shard_map/ppermute | solution.py:42
  33.8 13.8 %collective-permute-start.3 = (bf16[768,256]{1,0:T(8,128)(2,1)S(1)}, bf16[768,256]{1,0:T(8,128)(2,1)S(1)}, u32[]{:S(2)}, u32[]{:S(2)}) collective-permute-start(bf16[768,256]{1,0:T(8,128)(2,1)S(1)} %collective-permute-done.2), channel_id=1, source_target_pairs={{0,1},{1,2},{2,3},{3,4},{4,5},{5,6},{6,7},{7,0},{8,9},{9,10},{10,1... | collective-permute-start | bytes 1179656 | tf_op jit(solution)/shard_map/ppermute | solution.py:40
  36.6 67.1 %all-to-all-start = ((bf16[16,640,128]{1,2,0:T(8,128)(2,1)}), bf16[16,640,128]{1,2,0:T(8,128)(2,1)}, u32[]{:S(2)}, u32[]{:S(2)}) async-start(bf16[16,640,128]{1,2,0:T(8,128)(2,1)} %broadcast_in_dim.6), calls=%async_computation | async-start | bytes 5242880 | tf_op jit(solution)/shard_map/all_to_all | solution.py:20
  44.8 106.9 %reduce-scatter.4.cloned.1.call-start = ((), (), s32[]{:S(2)}) async-start(), calls=%async_computation.7 | async-start | bytes 3538944 | tf_op jit(solution)/shard_map/reduce_scatter | solution.py:73
  114.5 95.8 %all-gather.6.cloned.1.call-start = ((), (), s32[]{:S(2)}) async-start(), calls=%async_computation.8 | async-start | bytes 1671168 | tf_op jit(solution)/shard_map/all_gather | solution.py:15
  152.9 8.4 %collective-permute-start.7 = (bf16[768,256]{1,0:T(8,128)(2,1)S(1)}, bf16[768,256]{1,0:T(8,128)(2,1)S(1)}, u32[]{:S(2)}, u32[]{:S(2)}) collective-permute-start(bf16[768,256]{1,0:T(8,128)(2,1)S(1)} %add_convert_fusion.2), channel_id=1, source_target_pairs={{0,1},{1,2},{2,3},{3,4},{4,5},{5,6},{6,7},{7,0},{8,9},{9,10},{10,1... | collective-permute-start | bytes 1179656 | tf_op jit(solution)/shard_map/ppermute | solution.py:40
  161.3 8.4 %collective-permute-start.8 = (bf16[768,256]{1,0:T(8,128)(2,1)S(1)}, bf16[768,256]{1,0:T(8,128)(2,1)S(1)}, u32[]{:S(2)}, u32[]{:S(2)}) collective-permute-start(bf16[768,256]{1,0:T(8,128)(2,1)S(1)} %collective-permute-done.7), channel_id=1, source_target_pairs={{0,1},{1,2},{2,3},{3,4},{4,5},{5,6},{6,7},{7,0},{8,9},{9,10},{10,1... | collective-permute-start | bytes 1179656 | tf_op jit(solution)/shard_map/ppermute | solution.py:40
  169.7 8.4 %collective-permute-start.9 = (bf16[768,256]{1,0:T(8,128)(2,1)S(1)}, bf16[768,256]{1,0:T(8,128)(2,1)S(1)}, u32[]{:S(2)}, u32[]{:S(2)}) collective-permute-start(bf16[768,256]{1,0:T(8,128)(2,1)S(1)} %collective-permute-done.8), channel_id=1, source_target_pairs={{0,1},{1,2},{2,3},{3,4},{4,5},{5,6},{6,7},{7,0},{8,9},{9,10},{10,1... | collective-permute-start | bytes 1179656 | tf_op jit(solution)/shard_map/ppermute | solution.py:40
  170.3 16.2 %collective-permute-start.12 = (bf16[768,256]{1,0:T(8,128)(2,1)S(1)}, bf16[768,256]{1,0:T(8,128)(2,1)S(1)}, u32[]{:S(2)}, u32[]{:S(2)}) collective-permute-start(bf16[768,256]{1,0:T(8,128)(2,1)S(1)} %collective-permute-done.11), channel_id=1, source_target_pairs={{0,7},{1,0},{2,1},{3,2},{4,3},{5,4},{6,5},{7,6},{8,15},{9,8},{10,9... | collective-permute-start | bytes 1179656 | tf_op jit(solution)/shard_map/ppermute | solution.py:42
  178.1 11.0 %collective-permute-start.10 = (bf16[768,256]{1,0:T(8,128)(2,1)S(1)}, bf16[768,256]{1,0:T(8,128)(2,1)S(1)}, u32[]{:S(2)}, u32[]{:S(2)}) collective-permute-start(bf16[768,256]{1,0:T(8,128)(2,1)S(1)} %collective-permute-done.9), channel_id=1, source_target_pairs={{0,1},{1,2},{2,3},{3,4},{4,5},{5,6},{6,7},{7,0},{8,9},{9,10},{10,1... | collective-permute-start | bytes 1179656 | tf_op jit(solution)/shard_map/ppermute | solution.py:40
  179.2 36.1 %all-to-all-start.1 = ((bf16[16,128,128]{1,2,0:T(8,128)(2,1)}), bf16[16,128,128]{1,2,0:T(8,128)(2,1)}, u32[]{:S(2)}, u32[]{:S(2)}) async-start(bf16[16,128,128]{1,2,0:T(8,128)(2,1)} %broadcast_in_dim.7), calls=%async_computation.2 | async-start | bytes 1048576 | tf_op jit(solution)/shard_map/all_to_all | solution.py:20
  186.2 70.8 %reduce-scatter.6.cloned.1.call-start = ((), (), s32[]{:S(2)}) async-start(), calls=%async_computation.9 | async-start | bytes 3538944 | tf_op jit(solution)/shard_map/reduce_scatter | solution.py:73
  221.7 118.5 %all-gather.8.cloned.1.call-start = ((), (), s32[]{:S(2)}) async-start(), calls=%async_computation.10 | async-start | bytes 5570560 | tf_op jit(solution)/shard_map/all_gather | solution.py:15
  258.1 8.4 %collective-permute-start.14 = (bf16[768,256]{1,0:T(8,128)(2,1)S(1)}, bf16[768,256]{1,0:T(8,128)(2,1)S(1)}, u32[]{:S(2)}, u32[]{:S(2)}) collective-permute-start(bf16[768,256]{1,0:T(8,128)(2,1)S(1)} %add_convert_fusion.1), channel_id=1, source_target_pairs={{0,1},{1,2},{2,3},{3,4},{4,5},{5,6},{6,7},{7,0},{8,9},{9,10},{10,1... | collective-permute-start | bytes 1179656 | tf_op jit(solution)/shard_map/ppermute | solution.py:40
  266.5 8.4 %collective-permute-start.18 = (bf16[768,256]{1,0:T(8,128)(2,1)S(1)}, bf16[768,256]{1,0:T(8,128)(2,1)S(1)}, u32[]{:S(2)}, u32[]{:S(2)}) collective-permute-start(bf16[768,256]{1,0:T(8,128)(2,1)S(1)} %add_convert_fusion.1), channel_id=1, source_target_pairs={{0,7},{1,0},{2,1},{3,2},{4,3},{5,4},{6,5},{7,6},{8,15},{9,8},{10,9... | collective-permute-start | bytes 1179656 | tf_op jit(solution)/shard_map/ppermute | solution.py:42
  274.9 17.6 %collective-permute-start.19 = (bf16[768,256]{1,0:T(8,128)(2,1)S(1)}, bf16[768,256]{1,0:T(8,128)(2,1)S(1)}, u32[]{:S(2)}, u32[]{:S(2)}) collective-permute-start(bf16[768,256]{1,0:T(8,128)(2,1)S(1)} %collective-permute-done.18), channel_id=1, source_target_pairs={{0,7},{1,0},{2,1},{3,2},{4,3},{5,4},{6,5},{7,6},{8,15},{9,8},{10,9... | collective-permute-start | bytes 1179656 | tf_op jit(solution)/shard_map/ppermute | solution.py:42
  283.3 11.9 %collective-permute-start.17 = (bf16[768,256]{1,0:T(8,128)(2,1)S(1)}, bf16[768,256]{1,0:T(8,128)(2,1)S(1)}, u32[]{:S(2)}, u32[]{:S(2)}) collective-permute-start(bf16[768,256]{1,0:T(8,128)(2,1)S(1)} %collective-permute-done.16), channel_id=1, source_target_pairs={{0,1},{1,2},{2,3},{3,4},{4,5},{5,6},{6,7},{7,0},{8,9},{9,10},{10,1... | collective-permute-start | bytes 1179656 | tf_op jit(solution)/shard_map/ppermute | solution.py:40
  285.3 60.6 %all-to-all-start.2 = ((bf16[16,640,128]{1,2,0:T(8,128)(2,1)}), bf16[16,640,128]{1,2,0:T(8,128)(2,1)}, u32[]{:S(2)}, u32[]{:S(2)}) async-start(bf16[16,640,128]{1,2,0:T(8,128)(2,1)} %broadcast_in_dim.8), calls=%async_computation.4 | async-start | bytes 5242880 | tf_op jit(solution)/shard_map/all_to_all | solution.py:20
  292.3 103.8 %reduce-scatter.8.cloned.1.call-start = ((), (), s32[]{:S(2)}) async-start(), calls=%async_computation.11 | async-start | bytes 3538944 | tf_op jit(solution)/shard_map/reduce_scatter | solution.py:73
  (19 other events, 528.9 us)
Sparse Core Ops, SparseCore 0:
  9.5 88.4 all-gather.3
  114.6 37.1 reduce-scatter.3
  162.1 48.1 all-gather.5
  221.8 35.1 reduce-scatter.5
  259.0 81.1 all-gather.7
  356.8 39.3 reduce-scatter.7
